TPU v7x, 32 devices: a whole 2x2x4 slice. The times are simulated.
32 devices in a mesh: grp: 2 (over x), ep: 8 (over z, y), tp: 2 (over core).
Axes of the slice: x: 2, y: 2, z: 4, core: 2. Of those that a mesh axis runs over, the one named last changes fastest.
Arguments:
- tokens: bfloat16 [8192, 2048], P(('grp', 'ep', 'tp')), parts along dimension 0, may hold values from -6 to 6
- norm_gain: float32 [2048], replicated, may hold values from 0.1 to 1.9
- route_ids: int32 [8192, 2], P(('grp', 'ep', 'tp')), parts along dimension 0, may hold values from 0 to 7, as said below
- route_weights: float32 [8192, 2], P(('grp', 'ep', 'tp')), parts along dimension 0, may hold values from 0.1 to 1
- w_gate: bfloat16 [8, 2048, 512], P('ep', None, 'tp'), may hold values from -0.125 to 0.125
- w_up: bfloat16 [8, 2048, 512], P('ep', None, 'tp'), may hold values from -0.125 to 0.125
- w_down: bfloat16 [8, 512, 2048], P('ep', 'tp'), may hold values from -0.25 to 0.25
Outputs:
- mixed: bfloat16 [8192, 2048], P(('grp', 'ep', 'tp')), parts along dimension 0
There are 2 independent parts, one for each index of `grp`. A program takes and returns all parts, laid end to end along the dimension named above; an argument that names none is the same for every part. Nothing has to cross between parts.
Inputs may be any that keep to these rules, and one draw needn't show every extreme that they name: `route_ids`: the 2 experts of a token are different and lie in one group of 2 consecutive experts. Among the tokens of one device (aligned blocks of 256 tokens) no expert is named more than 128 times, and in every such block some expert is named exactly 128 times.
All inputs are finite; a program needn't handle non-finite values.
Results may differ from a plain program's by a relative error of at most 0.007.
Values may be sent and summed in bfloat16 or wider, within the bound.
A program may use at most 128 MiB of HBM per device.

v0:
```python
import jax
import jax.numpy as jnp
from jax import lax
from jax.sharding import PartitionSpec as P

GROUPS = 4


epsilon = 1e-06


def send_back(result):
    return lax.all_to_all(result, "ep", split_axis=0, concat_axis=0, tiled=True)


def per_device(tokens, norm_gain, route_ids, route_weights, w_gate, w_up, w_down):
    row_count, features = tokens.shape
    top_count = route_ids.shape[1]
    local_experts = w_gate.shape[0]
    ep_size = lax.axis_size("ep")
    experts_all = ep_size * local_experts
    capacity = row_count * GROUPS // experts_all
    floats = tokens.astype(jnp.float32)
    inverse = lax.rsqrt(jnp.mean(floats * floats, axis=1, keepdims=True) + epsilon)
    normed = (floats * inverse * norm_gain).astype(jnp.bfloat16)
    flat_ids = route_ids.reshape(-1)
    onehot = (flat_ids[:, None] == jnp.arange(experts_all, dtype=jnp.int32)[None, :]).astype(
        jnp.int32
    )
    earlier = jnp.cumsum(onehot, axis=0) - onehot
    slot_index = jnp.sum(earlier * onehot, axis=1)
    target = (flat_ids * capacity + slot_index).reshape(row_count, top_count)
    outbound = jnp.zeros((experts_all * capacity, features), jnp.bfloat16)
    for column in range(top_count):
        outbound = outbound.at[target[:, column]].set(normed)
    outbound = outbound.reshape(ep_size, local_experts, capacity, features)
    full_gate, full_up, full_down = (
        lax.all_gather(w_gate, "tp", axis=2, tiled=True),
        lax.all_gather(w_up, "tp", axis=2, tiled=True),
        lax.all_gather(w_down, "tp", axis=1, tiled=True),
    )
    arrived = lax.all_to_all(outbound, "ep", split_axis=0, concat_axis=0, tiled=True)
    gate_pre = jnp.einsum("sjcd,jdf->sjcf", arrived, full_gate, preferred_element_type=jnp.float32)
    up_pre = jnp.einsum("sjcd,jdf->sjcf", arrived, full_up, preferred_element_type=jnp.float32)
    hidden = (jax.nn.silu(gate_pre) * up_pre).astype(jnp.bfloat16)
    result = jnp.einsum("sjcf,jfd->sjcd", hidden, full_down, preferred_element_type=jnp.float32)
    returned_rows = send_back(result.astype(jnp.bfloat16))
    returned_rows = returned_rows.reshape(experts_all * capacity, features)
    combined = jnp.zeros((row_count, features), jnp.float32)
    for column in range(top_count):
        picked = returned_rows[target[:, column]].astype(jnp.float32)
        combined = combined + route_weights[:, column : column + 1] * picked
    return combined.astype(jnp.bfloat16)


def solution(mesh):
    in_specs = (
        P(("grp", "ep", "tp"), None),
        P(),
        P(("grp", "ep", "tp"), None),
        P(("grp", "ep", "tp"), None),
        P("ep", None, "tp"),
        P("ep", None, "tp"),
        P("ep", "tp", None),
    )
    out_specs = P(("grp", "ep", "tp"), None)
    return jax.shard_map(
        per_device, mesh=mesh, in_specs=in_specs, out_specs=out_specs, check_vma=False
    )
```

profile of v0, /device:TPU:9, one launch (start us, length us, event | category | flops | bytes accessed | tf_op | source)
XLA Modules:
  0.0 251.9 jit_solution(13313629162895466675)
XLA Ops:
  6.5 0.0 copy-start
  6.5 0.9 copy.22
  7.4 0.1 eq.29
  7.6 0.1 eq.25
  7.7 1.1 reduce-window.6
  8.9 0.2 slice_reduce_fusion
  9.1 0.1 fusion.34
  9.2 0.1 reduce_sum.21
  9.4 0.1 copy.24
  9.5 0.7 multiply_add_fusion
  10.2 1.5 fusion.4
  11.7 0.0 copy-done
  11.7 0.0 copy-start.1
  11.7 5.1 %scatter_custom_fusion = bf16[1024,2048]{1,0:T(8,128)(2,1)} fusion(s32[256]{0:T(256)S(1)} %bitcast.95, bf16[]{:T(256)} %constant.8.clone.1, bf16[256,2048]{1,0:T(8,128)(2,1)S(1)} %copy-done, f32[2048]{0:T(1024)} %param.8, f32[256]{0:T(256)S(1)} %add_rsqrt_fusion), kind=kCustom, calls=%fused_computation.25 | custom fusion | flops 2097152 | bytes 5252098 | tf_op jit(solution)/shard_map/scatter | solution.py:35
  16.9 0.0 copy-done.1
  16.9 7.2 %scatter_custom_fusion.1 = bf16[1024,2048]{1,0:T(8,128)(2,1)} fusion(bf16[1024,2048]{1,0:T(8,128)(2,1)} %scatter_custom_fusion, s32[256]{0:T(256)S(1)} %bitcast.93, bf16[256,2048]{1,0:T(8,128)(2,1)S(1)} %copy-done, f32[2048]{0:T(1024)S(1)} %copy-done.1, f32[256]{0:T(256)S(1)} %add_rsqrt_fusion), kind=kCustom, calls=%fused_computation.29 | custom fusion | flops 2097152 | bytes 5252096 | tf_op jit(solution)/shard_map/scatter | solution.py:35
  24.0 5.7 %all-to-all-start = ((bf16[8,1,128,2048]{3,2,1,0:T(8,128)(2,1)}), bf16[8,1,128,2048]{3,2,1,0:T(8,128)(2,1)}, u32[]{:S(2)}, u32[]{:S(2)}) async-start(bf16[8,1,128,2048]{3,2,1,0:T(8,128)(2,1)} %bitcast.90), calls=%async_computation | async-start | bytes 8388608 | tf_op jit(solution)/shard_map/all_to_all | solution.py:42
  29.7 0.0 all-gather.4.cloned.1.call-start
  29.7 0.7 all-gather.4.cloned.1.call-update
  30.5 0.0 all-gather.6.cloned.1.call-start
  30.5 0.7 all-gather.6.cloned.1.call-update
  31.2 0.2 all-gather.8.cloned.1.call-start
  31.4 0.5 all-gather.8.cloned.1.call-update
  31.9 12.4 %all-gather.4.cloned.1.call-done = bf16[1,2048,512]{2,1,0:T(8,128)(2,1)} async-done(((bf16[1,2048,256]{2,1,0:T(8,128)(2,1)}), bf16[1,2048,512]{2,1,0:T(8,128)(2,1)}) %all-gather.4.cloned.1.call-update) | async-done | bytes 2097168 | tf_op jit(solution)/shard_map/all_gather | solution.py:38
  44.4 76.8 %all-to-all-done = bf16[8,1,128,2048]{3,2,1,0:T(8,128)(2,1)} async-done(((bf16[8,1,128,2048]{3,2,1,0:T(8,128)(2,1)}), bf16[8,1,128,2048]{3,2,1,0:T(8,128)(2,1)}, u32[]{:S(2)}, u32[]{:S(2)}) %all-to-all-start) | async-done | bytes 4194336 | tf_op jit(solution)/shard_map/all_to_all | solution.py:42
  121.2 5.2 %fusion.2 = f32[8,128,512]{2,1,0:T(8,128)S(1)} fusion(bf16[8,1,128,2048]{3,2,1,0:T(8,128)(2,1)} %all-to-all-done, bf16[1,2048,512]{2,1,0:T(8,128)(2,1)} %all-gather.4.cloned.1.call-done), kind=kOutput, calls=%fused_computation.6 | convolution fusion | flops 2147483648 | bytes 8388608 | tf_op jit(solution)/shard_map/sjcd,jdf->sjcf/dot_general | solution.py:43
  126.4 0.0 all-gather.6.cloned.1.call-done
  126.4 0.0 all-gather.8.cloned.1.call-done
  126.4 10.1 %convert_bitcast_fusion = bf16[8,1,128,2048]{3,2,1,0:T(8,128)(2,1)} fusion(bf16[1,512,2048]{2,1,0:T(8,128)(2,1)} %all-gather.8.cloned.1.call-done, bf16[1,2048,512]{2,1,0:T(8,128)(2,1)} %all-gather.6.cloned.1.call-done, bf16[8,1,128,2048]{3,2,1,0:T(8,128)(2,1)} %all-to-all-done, f32[8,128,512]{2,1,0:T(8,128)S(1)} %fusion.2), kind=kOutput, calls=%fused_computation.8 | convolution fusion | flops 4300210176 | bytes 14680064 | tf_op jit(solution)/shard_map/sjcf,jfd->sjcd/dot_general | solution.py:46
  136.5 0.0 copy-start.2
  136.5 5.8 %all-to-all-start.1 = ((bf16[8,1,128,2048]{3,2,1,0:T(8,128)(2,1)}), bf16[8,1,128,2048]{3,2,1,0:T(8,128)(2,1)}, u32[]{:S(2)}, u32[]{:S(2)}) async-start(bf16[8,1,128,2048]{3,2,1,0:T(8,128)(2,1)} %convert_bitcast_fusion), calls=%async_computation.1 | async-start | bytes 8388608 | tf_op jit(solution)/shard_map/all_to_all | solution.py:13
  142.3 0.0 copy-done.2
  142.3 91.4 %all-to-all-done.1 = bf16[8,1,128,2048]{3,2,1,0:T(8,128)(2,1)} async-done(((bf16[8,1,128,2048]{3,2,1,0:T(8,128)(2,1)}), bf16[8,1,128,2048]{3,2,1,0:T(8,128)(2,1)}, u32[]{:S(2)}, u32[]{:S(2)}) %all-to-all-start.1) | async-done | bytes 4194336 | tf_op jit(solution)/shard_map/all_to_all | solution.py:13
  233.7 5.1 %gather_fusion = bf16[256,2048]{1,0:T(8,128)(2,1)S(1)} fusion(bf16[1024,2048]{1,0:T(8,128)(2,1)} %bitcast.27, s32[1024]{0:T(1024)S(1)} %pad_clamp_fusion.1), kind=kCustom, calls=%fused_computation | custom fusion | bytes 2098176 | tf_op jit(solution)/shard_map/gather | solution.py:51
  238.8 5.1 %gather_fusion.1 = bf16[256,2048]{1,0:T(8,128)(2,1)S(1)} fusion(bf16[1024,2048]{1,0:T(8,128)(2,1)} %bitcast.27, s32[1024]{0:T(1024)S(1)} %pad_clamp_fusion), kind=kCustom, calls=%fused_computation.1 | custom fusion | bytes 2098176 | tf_op jit(solution)/shard_map/gather | solution.py:51
  243.9 1.4 add_convert_fusion
  (8 shorter events, 0.1 us)
Async XLA Ops:
  6.5 5.2 %copy-start = (bf16[256,2048]{1,0:T(8,128)(2,1)S(1)}, bf16[256,2048]{1,0:T(8,128)(2,1)}, u32[]{:S(2)}) copy-start(bf16[256,2048]{1,0:T(8,128)(2,1)} %param.7) | copy-start | bytes 3145732
  11.7 5.1 %copy-start.1 = (f32[2048]{0:T(1024)S(1)}, f32[2048]{0:T(1024)}, u32[]{:S(2)}) copy-start(f32[2048]{0:T(1024)} %param.8) | copy-start | bytes 24580
  24.0 97.2 %all-to-all-start = ((bf16[8,1,128,2048]{3,2,1,0:T(8,128)(2,1)}), bf16[8,1,128,2048]{3,2,1,0:T(8,128)(2,1)}, u32[]{:S(2)}, u32[]{:S(2)}) async-start(bf16[8,1,128,2048]{3,2,1,0:T(8,128)(2,1)} %bitcast.90), calls=%async_computation | async-start | bytes 8388608 | tf_op jit(solution)/shard_map/all_to_all | solution.py:42
  29.7 14.6 %all-gather.4.cloned.1.call-start = ((), (), s32[]{:S(2)}) async-start(), calls=%async_computation.2 | async-start | bytes 3145728 | tf_op jit(solution)/shard_map/all_gather | solution.py:38
  30.5 96.0 %all-gather.6.cloned.1.call-start = ((), (), s32[]{:S(2)}) async-start(), calls=%async_computation.3 | async-start | bytes 3145728 | tf_op jit(solution)/shard_map/all_gather | solution.py:39
  31.2 95.2 %all-gather.8.cloned.1.call-start = ((), (), s32[]{:S(2)}) async-start(), calls=%async_computation.4 | async-start | bytes 3145728 | tf_op jit(solution)/shard_map/all_gather | solution.py:40
  136.5 5.8 %copy-start.2 = (f32[256,2]{0,1:T(2,128)S(1)}, f32[256,2]{0,1:T(2,128)}, u32[]{:S(2)}) copy-start(f32[256,2]{0,1:T(2,128)} %param.10) | copy-start | bytes 6148
  136.5 97.2 %all-to-all-start.1 = ((bf16[8,1,128,2048]{3,2,1,0:T(8,128)(2,1)}), bf16[8,1,128,2048]{3,2,1,0:T(8,128)(2,1)}, u32[]{:S(2)}, u32[]{:S(2)}) async-start(bf16[8,1,128,2048]{3,2,1,0:T(8,128)(2,1)} %convert_bitcast_fusion), calls=%async_computation.1 | async-start | bytes 8388608 | tf_op jit(solution)/shard_map/all_to_all | solution.py:13
Sparse Core Ops, SparseCore 0:
  32.1 12.2 all-gather.3
  45.9 11.2 all-gather.5
  58.8 11.7 all-gather.7
where the time goes:
time: 256 us; the launch traced here: 252 us
  waiting for transfers between devices  183 us (71%)
  other arithmetic  17.2 us (7%)
  matrix products  15.3 us (6%)
  between operations  13.2 us (5%)
  local copies, waits for them, and re-layouts  11.8 us (5%)
  starting transfers between devices  11.7 us (5%)
    all_to_all x1, waiting for transfers between devices, send_back(): return lax.all_to_all(result, 'ep', split_axis=0, concat_axis=0, tiled=True)  91.4 us
    all_to_all x1, waiting for transfers between devices, per_device(): lax.all_to_all(outbound, 'ep', split_axis=0, concat_axis=0, tiled=True)  76.8 us
    all_gather x1, waiting for transfers between devices, per_device(): lax.all_gather(w_gate, 'tp', axis=2, tiled=True)  12.4 us
    scatter x2, other arithmetic, per_device(): outbound = outbound.at[target[:, column]].set(normed)  12.3 us
    gather x2, local copies, waits for them, and re-layouts, per_device(): picked = returned_rows[target[:, column]].astype(jnp.float32)  10.2 us
    dot_general x1, matrix products, per_device(): jnp.einsum('sjcf,jfd->sjcd', hidden, full_down, preferred_element_type=jn...  10.1 us
    all_to_all x1, starting transfers between devices, send_back(): return lax.all_to_all(result, 'ep', split_axis=0, concat_axis=0, tiled=True)  5.76 us
    all_to_all x1, starting transfers between devices, per_device(): lax.all_to_all(outbound, 'ep', split_axis=0, concat_axis=0, tiled=True)  5.72 us
  transfers between devices with their start and end apart: 5, of which 3 were waited for; matrix products, arithmetic and copies ran while one was open for 2% of the time, Pallas kernels for 0%

commit v1 on v0

--- a/solution.py
+++ b/solution.py
@@ -1,9 +1,15 @@
+import functools
+
 import jax
 import jax.numpy as jnp
 from jax import lax
+from jax.experimental import pallas as pl
+from jax.experimental.pallas import tpu as pltpu
 from jax.sharding import PartitionSpec as P
 
 GROUPS = 4
+SPLIT = 2
+MESH = pl.DeviceIdType.MESH
 
 
 epsilon = 1e-06
@@ -13,7 +19,7 @@
     return lax.all_to_all(result, "ep", split_axis=0, concat_axis=0, tiled=True)
 
 
-def per_device(tokens, norm_gain, route_ids, route_weights, w_gate, w_up, w_down):
+def general_layer(tokens, norm_gain, route_ids, route_weights, w_gate, w_up, w_down):
     row_count, features = tokens.shape
     top_count = route_ids.shape[1]
     local_experts = w_gate.shape[0]
@@ -53,7 +59,279 @@
     return combined.astype(jnp.bfloat16)
 
 
+def group_kernel(
+    members, parts, halves,
+    tokens, gain, ids, weights, w_gate, w_up, w_down, out,
+    normed, place, sent, taken, scales, scales_in, answers, returned,
+    gate_all, up_all, down_all, hidden,
+    own_sems, twin_s, twin_r, peer_s, peer_r, part_s, part_r,
+    near_s, near_r, far_s, far_r, row_s, row_r, scale_s, scale_r, back_s, back_r,
+):
+    part, position, half = lax.axis_index("grp"), lax.axis_index("ep"), lax.axis_index("tp")
+    level, member = position // members, position % members
+    rows, features = tokens.shape
+    slots = sent.shape[1]
+    top_count = ids.shape[0]
+    peer = {"ep": level * members + (members - 1 - member)}
+    other_part = {"grp": parts - 1 - part}
+    twin = {"tp": halves - 1 - half}
+
+    def level_of(k):
+        return {"ep": (level ^ k) * members + member}
+
+    barrier = pltpu.get_barrier_semaphore()
+    neighbours = [peer, other_part, twin] + [level_of(k) for k in range(1, GROUPS)]
+    for device in neighbours:
+        pl.semaphore_signal(barrier, inc=1, device_id=device, device_id_type=MESH)
+    pl.semaphore_wait(barrier, len(neighbours))
+
+    sources = (w_gate, w_up, w_down)
+    stores = (gate_all, up_all, down_all)
+    mine = member * halves + half
+    theirs = (members - 1 - member) * halves + half
+
+    def remote(src, dst, send, recv, device):
+        return pltpu.make_async_remote_copy(
+            src_ref=src, dst_ref=dst, send_sem=send, recv_sem=recv,
+            device_id=device, device_id_type=MESH,
+        )
+
+    pieces = []
+    for step in range(SPLIT):
+        for tensor in range(3):
+            size = sources[tensor].shape[0] // (parts * SPLIT)
+            pieces.append((tensor, step, size))
+
+    def span(index, which):
+        tensor, step, size = pieces[index]
+        start = pl.multiple_of((which * SPLIT + step) * size, size)
+        return tensor, pl.ds(start, size)
+
+    def peer_copy(index):
+        tensor, window = span(index, part)
+        return remote(
+            sources[tensor].at[window], stores[tensor].at[mine, window],
+            peer_s.at[index], peer_r.at[index], peer,
+        )
+
+    def spread_copy(index, which, send, recv, device):
+        tensor, window = span(index, which)
+        block = stores[tensor].at[theirs, window]
+        return remote(block, block, send.at[index], recv.at[index], device)
+
+    peer_copies = [peer_copy(index) for index in range(len(pieces))]
+    part_copies = [spread_copy(i, part, part_s, part_r, other_part) for i in range(len(pieces))]
+    near_copies = [spread_copy(i, part, near_s, near_r, twin) for i in range(len(pieces))]
+    far_copies = [
+        spread_copy(i, parts - 1 - part, far_s, far_r, twin) for i in range(len(pieces))
+    ]
+    for copy in peer_copies:
+        copy.start()
+    own_copies, twin_copies = [], []
+    for tensor in range(3):
+        own_copies.append(
+            pltpu.make_async_copy(sources[tensor], stores[tensor].at[mine], own_sems.at[tensor])
+        )
+        twin_copies.append(
+            remote(
+                sources[tensor], stores[tensor].at[mine],
+                twin_s.at[tensor], twin_r.at[tensor], twin,
+            )
+        )
+    for copy in own_copies + twin_copies:
+        copy.start()
+
+    strip = 32
+
+    def norm_strip(index, carry):
+        window = pl.ds(pl.multiple_of(index * strip, strip), strip)
+        floats = tokens[window, :].astype(jnp.float32)
+        inverse = lax.rsqrt(jnp.mean(floats * floats, axis=1, keepdims=True) + epsilon)
+        normed[window, :] = (floats * inverse * gain[...]).astype(jnp.bfloat16)
+        return carry
+
+    lax.fori_loop(0, rows // strip, norm_strip, 0)
+
+    first = ids[0:1, :]
+    group_row = first // members
+    lane = lax.broadcasted_iota(jnp.int32, (8, rows), 0)
+    mask = (jnp.broadcast_to(group_row, (8, rows)) == lane).astype(jnp.float32)
+    before = (
+        lax.broadcasted_iota(jnp.int32, (rows, rows), 0)
+        < lax.broadcasted_iota(jnp.int32, (rows, rows), 1)
+    ).astype(jnp.float32)
+    ranks = jnp.dot(
+        mask.astype(jnp.bfloat16), before.astype(jnp.bfloat16),
+        preferred_element_type=jnp.float32,
+    )
+    slot_row = jnp.sum(ranks * mask, axis=0, keepdims=True).astype(jnp.int32)
+    shares = jnp.zeros((8, rows), jnp.float32)
+    for column in range(top_count):
+        offset = ids[column : column + 1, :] - group_row * members
+        chosen = jnp.broadcast_to(offset, (8, rows)) == lane
+        shares = shares + jnp.where(
+            chosen, jnp.broadcast_to(weights[column : column + 1, :], (8, rows)), 0.0
+        )
+    high = shares.astype(jnp.bfloat16)
+    rest = shares - high.astype(jnp.float32)
+    middle = rest.astype(jnp.bfloat16)
+    low = (rest - middle.astype(jnp.float32)).astype(jnp.bfloat16)
+
+    row_copies, scale_copies, back_copies = {}, {}, {}
+    slot_iota = lax.broadcasted_iota(jnp.int32, (slots, rows), 0)
+    order = [2, 3, 1, 0]
+    for k in order:
+        key = jnp.where(group_row == (level ^ k), slot_row, -1)
+        spots = (jnp.broadcast_to(key, (slots, rows)) == slot_iota).astype(jnp.float32)
+        spots = spots.astype(jnp.bfloat16)
+        place[k * slots : (k + 1) * slots, :] = spots
+        lanes = sum(
+            lax.dot_general(
+                piece, spots, (((1,), (1,)), ((), ())), preferred_element_type=jnp.float32
+            )
+            for piece in (high, middle, low)
+        )
+        packed = taken if k == 0 else sent
+        (scales_in if k == 0 else scales)[k] = lanes
+        packed[k] = jnp.dot(spots, normed[...], preferred_element_type=jnp.float32).astype(
+            jnp.bfloat16
+        )
+        if k:
+            row_copies[k] = remote(sent.at[k], taken.at[k], row_s.at[k], row_r.at[k], level_of(k))
+            scale_copies[k] = remote(
+                scales.at[k], scales_in.at[k], scale_s.at[k], scale_r.at[k], level_of(k)
+            )
+            row_copies[k].start()
+            scale_copies[k].start()
+
+    for index in range(len(pieces)):
+        peer_copies[index].wait_recv()
+        part_copies[index].start()
+        near_copies[index].start()
+        if index:
+            part_copies[index - 1].wait_recv()
+            far_copies[index - 1].start()
+    part_copies[-1].wait_recv()
+    far_copies[-1].start()
+    for copy in own_copies:
+        copy.wait()
+    for copy in twin_copies + near_copies + far_copies:
+        copy.wait_recv()
+
+    width = gate_all.shape[2]
+    diagonal = lax.broadcasted_iota(jnp.int32, (slots, slots), 0) == lax.broadcasted_iota(
+        jnp.int32, (slots, slots), 1
+    )
+    tile = 512
+
+    def work(k):
+        for block in range(members * halves):
+            lanes = scales_in[k][block // halves : block // halves + 1, :]
+            scale = jnp.sum(
+                jnp.where(diagonal, jnp.broadcast_to(lanes, (slots, slots)), 0.0),
+                axis=1, keepdims=True,
+            )
+            gate = jnp.dot(taken[k], gate_all[block], preferred_element_type=jnp.float32)
+            up = jnp.dot(taken[k], up_all[block], preferred_element_type=jnp.float32)
+            hidden[:, block * width : (block + 1) * width] = (
+                gate / (1.0 + jnp.exp(-gate)) * up * scale
+            ).astype(jnp.bfloat16)
+        for column in range(features // tile):
+            window = slice(column * tile, (column + 1) * tile)
+            total = jnp.zeros((slots, tile), jnp.float32)
+            for block in range(members * halves):
+                total += jnp.dot(
+                    hidden[:, block * width : (block + 1) * width],
+                    down_all[block, :, window],
+                    preferred_element_type=jnp.float32,
+                )
+            if k:
+                answers[k, :, window] = total.astype(jnp.bfloat16)
+            else:
+                returned[0, :, window] = total.astype(jnp.bfloat16)
+
+    for k in (2, 3, 1, 0):
+        if k:
+            row_copies[k].wait_recv()
+            scale_copies[k].wait_recv()
+        work(k)
+        if k:
+            back_copies[k] = remote(
+                answers.at[k], returned.at[k], back_s.at[k], back_r.at[k], level_of(k)
+            )
+            back_copies[k].start()
+
+    for k in (1, 2, 3):
+        back_copies[k].wait_recv()
+    for column in range(features // tile):
+        window = slice(column * tile, (column + 1) * tile)
+        total = jnp.zeros((rows, tile), jnp.float32)
+        for k in range(GROUPS):
+            total += lax.dot_general(
+                place[k * slots : (k + 1) * slots, :], returned[k, :, window],
+                (((0,), (0,)), ((), ())), preferred_element_type=jnp.float32,
+            )
+        out[:, window] = total.astype(jnp.bfloat16)
+
+    for copy in peer_copies + part_copies + near_copies + far_copies + twin_copies:
+        copy.wait_send()
+    for k in (1, 2, 3):
+        row_copies[k].wait_send()
+        scale_copies[k].wait_send()
+        back_copies[k].wait_send()
+
+
+def group_layer(members, tokens, norm_gain, route_ids, route_weights, w_gate, w_up, w_down):
+    rows, features = tokens.shape
+    parts, halves = lax.axis_size("grp"), lax.axis_size("tp")
+    width = w_gate.shape[2]
+    slots = rows // route_ids.shape[1]
+    copies = 3 * SPLIT
+    blocks = members * halves
+    bf16, f32, dma = jnp.bfloat16, jnp.float32, pltpu.SemaphoreType.DMA
+    vmem, anywhere = pl.BlockSpec(memory_space=pltpu.VMEM), pl.BlockSpec(memory_space=pl.ANY)
+    return pl.pallas_call(
+        functools.partial(group_kernel, members, parts, halves),
+        out_shape=jax.ShapeDtypeStruct((rows, features), bf16),
+        in_specs=[vmem] * 4 + [anywhere] * 3,
+        out_specs=vmem,
+        scratch_shapes=[
+            pltpu.VMEM((rows, features), bf16),
+            pltpu.VMEM((GROUPS * slots, rows), bf16),
+            pltpu.VMEM((GROUPS, slots, features), bf16),
+            pltpu.VMEM((GROUPS, slots, features), bf16),
+            pltpu.VMEM((GROUPS, 8, slots), f32),
+            pltpu.VMEM((GROUPS, 8, slots), f32),
+            pltpu.VMEM((GROUPS, slots, features), bf16),
+            pltpu.VMEM((GROUPS, slots, features), bf16),
+            pltpu.VMEM((blocks, features, width), bf16),
+            pltpu.VMEM((blocks, features, width), bf16),
+            pltpu.VMEM((blocks, width, features), bf16),
+            pltpu.VMEM((slots, blocks * width), bf16),
+            dma((3,)), dma((3,)), dma((3,)),
+        ]
+        + [dma((copies,)) for _ in range(8)]
+        + [dma((GROUPS,)) for _ in range(6)],
+        compiler_params=pltpu.CompilerParams(
+            collective_id=0, has_side_effects=True, vmem_limit_bytes=48 * 1024 * 1024
+        ),
+    )(
+        tokens, norm_gain.reshape(1, features), route_ids.T, route_weights.T,
+        w_gate[0], w_up[0], w_down[0],
+    )
+
+
 def solution(mesh):
+    sizes = mesh.shape
+
+    def per_device(tokens, norm_gain, route_ids, route_weights, w_gate, w_up, w_down):
+        arguments = (tokens, norm_gain, route_ids, route_weights, w_gate, w_up, w_down)
+        members = sizes["ep"] * w_gate.shape[0] // GROUPS
+        paired = members == route_ids.shape[1] == sizes["grp"] == sizes["tp"] == 2
+        if paired and w_gate.shape[0] == 1:
+            return group_layer(members, *arguments)
+        return general_layer(*arguments)
+
     in_specs = (
         P(("grp", "ep", "tp"), None),
         P(),

time: 256 us -> 107 us (0.42)
  waiting for transfers between devices: 183 us -> 0 us
  Pallas kernels: 0 us -> 97.2 us
  other arithmetic: 17.2 us -> 0 us
  matrix products: 15.3 us -> 0 us
  between operations: 13.2 us -> 0.02 us
  starting transfers between devices: 11.7 us -> 0 us
  local copies, waits for them, and re-layouts: 11.8 us -> 7.25 us
    all_to_all x2 -> x0, waiting for transfers between devices: 168 us -> none  [the longest x1 91.4 us: send_back(): return lax.all_to_all(result, 'ep', split_axis=0, concat_axis=0, tiled=True)]
    pallas_call x0 -> x1, Pallas kernels: none -> 97.2 us  [group_layer(): pl.pallas_call(functools.partial(group_kernel, members, parts, halves), o...]
    dot_general x2 -> x0, matrix products: 15.3 us -> none  [the longest x1 10.1 us: per_device(): jnp.einsum('sjcf,jfd->sjcd', hidden, full_down, preferred_element_type=jn...]
    all_gather x3 -> x0, waiting for transfers between devices: 12.5 us -> none  [the longest x1 12.4 us: per_device(): lax.all_gather(w_gate, 'tp', axis=2, tiled=True)]
    scatter x2 -> x0, other arithmetic: 12.3 us -> none  [per_device(): outbound = outbound.at[target[:, column]].set(normed)]
    all_to_all x2 -> x0, starting transfers between devices: 11.5 us -> none  [the longest x1 5.76 us: send_back(): return lax.all_to_all(result, 'ep', split_axis=0, concat_axis=0, tiled=True)]
    gather x2 -> x0, local copies, waits for them, and re-layouts: 10.2 us -> none  [per_device(): picked = returned_rows[target[:, column]].astype(jnp.float32)]
    unnamed x7 -> x15, local copies, waits for them, and re-layouts: 0.91 us -> 7.25 us
  transfers between devices with their start and end apart: 5 -> 0, of which waited for: 3 -> 0; matrix products, arithmetic and copies ran while one was open for 2% -> 0% of each run, Pallas kernels for 0% -> 0%
where the time goes in v1:
time: 107 us; the launch traced here: 105 us
  Pallas kernels  97.2 us (91%)
  local copies, waits for them, and re-layouts  7.25 us (7%)
    pallas_call x1, Pallas kernels, group_layer(): pl.pallas_call(functools.partial(group_kernel, members, parts, halves), o...  97.2 us
    unnamed x15, local copies, waits for them, and re-layouts  7.25 us

profile of v1, /device:TPU:9, one launch (start us, length us, event | category | flops | bytes accessed | tf_op | source)
XLA Modules:
  0.0 104.5 jit_solution(11452928999146314319)
XLA Ops:
  0.0 0.0 copy-start.4
  0.0 0.0 copy-start.5
  0.0 0.7 copy-done.4
  0.7 0.0 copy-done.5
  0.7 0.0 copy-start
  0.7 1.2 %copy-done = bf16[256,2048]{1,0:T(8,128)(2,1)S(1)} copy-done((bf16[256,2048]{1,0:T(8,128)(2,1)S(1)}, bf16[256,2048]{1,0:T(8,128)(2,1)}, u32[]{:S(2)}) %copy-start) | copy-done | bytes 1048600
  1.9 0.0 copy-start.1
  1.9 1.2 %copy-done.1 = bf16[1,2048,256]{2,1,0:T(8,128)(2,1)S(1)} copy-done((bf16[1,2048,256]{2,1,0:T(8,128)(2,1)S(1)}, bf16[1,2048,256]{2,1,0:T(8,128)(2,1)}, u32[]{:S(2)}) %copy-start.1) | copy-done | bytes 1048600
  3.2 0.0 copy-start.2
  3.2 1.2 %copy-done.2 = bf16[1,2048,256]{2,1,0:T(8,128)(2,1)S(1)} copy-done((bf16[1,2048,256]{2,1,0:T(8,128)(2,1)S(1)}, bf16[1,2048,256]{2,1,0:T(8,128)(2,1)}, u32[]{:S(2)}) %copy-start.2) | copy-done | bytes 1048600
  4.4 0.0 copy-start.3
  4.4 1.2 %copy-done.3 = bf16[1,256,2048]{2,1,0:T(8,128)(2,1)S(1)} copy-done((bf16[1,256,2048]{2,1,0:T(8,128)(2,1)S(1)}, bf16[1,256,2048]{2,1,0:T(8,128)(2,1)}, u32[]{:S(2)}) %copy-start.3) | copy-done | bytes 1048600
  5.6 0.0 copy-start.6
  5.6 0.7 copy-done.6
  6.3 97.2 %shard_map.73 = bf16[256,2048]{1,0:T(8,128)(2,1)S(1)} custom-call(bf16[256,2048]{1,0:T(8,128)(2,1)S(1)} %copy-done, f32[1,2048]{1,0:T(1,128)S(1)} %bitcast.9, s32[2,256]{1,0:T(2,128)S(1)} %bitcast.10, f32[2,256]{1,0:T(2,128)S(1)} %bitcast.11, bf16[2048,256]{1,0:T(8,128)(2,1)S(1)} %bitcast.6, bf16[2048,256]{1,0:T(8,128)(2,1)S(1)} %bitcast.7, ...), custom_call_target="tpu_custom_call" | custom-call | tf_op jit(solution)/shard_map/pallas_call | solution.py:293
  103.5 1.0 copy.9
Async XLA Ops:
  0.0 0.7 copy-start.4
  0.0 0.7 copy-start.5
  0.7 1.2 %copy-start = (bf16[256,2048]{1,0:T(8,128)(2,1)S(1)}, bf16[256,2048]{1,0:T(8,128)(2,1)}, u32[]{:S(2)}) copy-start(bf16[256,2048]{1,0:T(8,128)(2,1)} %tokens.1) | copy-start | bytes 3145732
  1.9 1.2 %copy-start.1 = (bf16[1,2048,256]{2,1,0:T(8,128)(2,1)S(1)}, bf16[1,2048,256]{2,1,0:T(8,128)(2,1)}, u32[]{:S(2)}) copy-start(bf16[1,2048,256]{2,1,0:T(8,128)(2,1)} %param.11) | copy-start | bytes 3145732
  3.2 1.2 %copy-start.2 = (bf16[1,2048,256]{2,1,0:T(8,128)(2,1)S(1)}, bf16[1,2048,256]{2,1,0:T(8,128)(2,1)}, u32[]{:S(2)}) copy-start(bf16[1,2048,256]{2,1,0:T(8,128)(2,1)} %param.12) | copy-start | bytes 3145732
  4.4 1.2 %copy-start.3 = (bf16[1,256,2048]{2,1,0:T(8,128)(2,1)S(1)}, bf16[1,256,2048]{2,1,0:T(8,128)(2,1)}, u32[]{:S(2)}) copy-start(bf16[1,256,2048]{2,1,0:T(8,128)(2,1)} %param.13) | copy-start | bytes 3145732
  5.6 0.7 copy-start.6

commit v2 on v1

--- a/solution.py
+++ b/solution.py
@@ -62,9 +62,9 @@
 def group_kernel(
     members, parts, halves,
     tokens, gain, ids, weights, w_gate, w_up, w_down, out,
-    normed, place, sent, taken, scales, scales_in, answers, returned,
+    raw, ready, summed, place, sent, taken, scales, scales_in, answers, returned,
     gate_all, up_all, down_all, hidden,
-    own_sems, twin_s, twin_r, peer_s, peer_r, part_s, part_r,
+    raw_sem, own_sems, twin_s, twin_r, peer_s, peer_r, part_s, part_r,
     near_s, near_r, far_s, far_r, row_s, row_r, scale_s, scale_r, back_s, back_r,
 ):
     part, position, half = lax.axis_index("grp"), lax.axis_index("ep"), lax.axis_index("tp")
@@ -79,6 +79,8 @@
     def level_of(k):
         return {"ep": (level ^ k) * members + member}
 
+    raw_copy = pltpu.make_async_copy(tokens, raw, raw_sem)
+    raw_copy.start()
     barrier = pltpu.get_barrier_semaphore()
     neighbours = [peer, other_part, twin] + [level_of(k) for k in range(1, GROUPS)]
     for device in neighbours:
@@ -141,17 +143,6 @@
     for copy in own_copies + twin_copies:
         copy.start()
 
-    strip = 32
-
-    def norm_strip(index, carry):
-        window = pl.ds(pl.multiple_of(index * strip, strip), strip)
-        floats = tokens[window, :].astype(jnp.float32)
-        inverse = lax.rsqrt(jnp.mean(floats * floats, axis=1, keepdims=True) + epsilon)
-        normed[window, :] = (floats * inverse * gain[...]).astype(jnp.bfloat16)
-        return carry
-
-    lax.fori_loop(0, rows // strip, norm_strip, 0)
-
     first = ids[0:1, :]
     group_row = first // members
     lane = lax.broadcasted_iota(jnp.int32, (8, rows), 0)
@@ -179,7 +170,8 @@
 
     row_copies, scale_copies, back_copies = {}, {}, {}
     slot_iota = lax.broadcasted_iota(jnp.int32, (slots, rows), 0)
-    order = [2, 3, 1, 0]
+    raw_copy.wait()
+    order = (2, 1, 3, 0)
     for k in order:
         key = jnp.where(group_row == (level ^ k), slot_row, -1)
         spots = (jnp.broadcast_to(key, (slots, rows)) == slot_iota).astype(jnp.float32)
@@ -193,7 +185,7 @@
         )
         packed = taken if k == 0 else sent
         (scales_in if k == 0 else scales)[k] = lanes
-        packed[k] = jnp.dot(spots, normed[...], preferred_element_type=jnp.float32).astype(
+        packed[k] = jnp.dot(spots, raw[...], preferred_element_type=jnp.float32).astype(
             jnp.bfloat16
         )
         if k:
@@ -224,15 +216,25 @@
     )
     tile = 512
 
+    strip = 32
+
     def work(k):
+        def norm_strip(index, carry):
+            window = pl.ds(pl.multiple_of(index * strip, strip), strip)
+            floats = taken[k, window, :].astype(jnp.float32)
+            inverse = lax.rsqrt(jnp.mean(floats * floats, axis=1, keepdims=True) + epsilon)
+            ready[window, :] = (floats * inverse * gain[...]).astype(jnp.bfloat16)
+            return carry
+
+        lax.fori_loop(0, slots // strip, norm_strip, 0)
         for block in range(members * halves):
             lanes = scales_in[k][block // halves : block // halves + 1, :]
             scale = jnp.sum(
                 jnp.where(diagonal, jnp.broadcast_to(lanes, (slots, slots)), 0.0),
                 axis=1, keepdims=True,
             )
-            gate = jnp.dot(taken[k], gate_all[block], preferred_element_type=jnp.float32)
-            up = jnp.dot(taken[k], up_all[block], preferred_element_type=jnp.float32)
+            gate = jnp.dot(ready[...], gate_all[block], preferred_element_type=jnp.float32)
+            up = jnp.dot(ready[...], up_all[block], preferred_element_type=jnp.float32)
             hidden[:, block * width : (block + 1) * width] = (
                 gate / (1.0 + jnp.exp(-gate)) * up * scale
             ).astype(jnp.bfloat16)
@@ -250,7 +252,7 @@
             else:
                 returned[0, :, window] = total.astype(jnp.bfloat16)
 
-    for k in (2, 3, 1, 0):
+    for k in order:
         if k:
             row_copies[k].wait_recv()
             scale_copies[k].wait_recv()
@@ -261,17 +263,23 @@
             )
             back_copies[k].start()
 
-    for k in (1, 2, 3):
+    def unpack(k, window):
+        return lax.dot_general(
+            place[k * slots : (k + 1) * slots, :], returned[k, :, window],
+            (((0,), (0,)), ((), ())), preferred_element_type=jnp.float32,
+        )
+
+    tiles = [slice(start, start + tile) for start in range(0, features, tile)]
+    for window in tiles:
+        summed[:, window] = unpack(0, window)
+    for k in order[:-1]:
         back_copies[k].wait_recv()
-    for column in range(features // tile):
-        window = slice(column * tile, (column + 1) * tile)
-        total = jnp.zeros((rows, tile), jnp.float32)
-        for k in range(GROUPS):
-            total += lax.dot_general(
-                place[k * slots : (k + 1) * slots, :], returned[k, :, window],
-                (((0,), (0,)), ((), ())), preferred_element_type=jnp.float32,
-            )
-        out[:, window] = total.astype(jnp.bfloat16)
+        for window in tiles:
+            total = summed[:, window] + unpack(k, window)
+            if k == order[-2]:
+                out[:, window] = total.astype(jnp.bfloat16)
+            else:
+                summed[:, window] = total
 
     for copy in peer_copies + part_copies + near_copies + far_copies + twin_copies:
         copy.wait_send()
@@ -293,10 +301,12 @@
     return pl.pallas_call(
         functools.partial(group_kernel, members, parts, halves),
         out_shape=jax.ShapeDtypeStruct((rows, features), bf16),
-        in_specs=[vmem] * 4 + [anywhere] * 3,
+        in_specs=[anywhere] + [vmem] * 3 + [anywhere] * 3,
         out_specs=vmem,
         scratch_shapes=[
             pltpu.VMEM((rows, features), bf16),
+            pltpu.VMEM((slots, features), bf16),
+            pltpu.VMEM((rows, features), f32),
             pltpu.VMEM((GROUPS * slots, rows), bf16),
             pltpu.VMEM((GROUPS, slots, features), bf16),
             pltpu.VMEM((GROUPS, slots, features), bf16),
@@ -308,12 +318,12 @@
             pltpu.VMEM((blocks, features, width), bf16),
             pltpu.VMEM((blocks, width, features), bf16),
             pltpu.VMEM((slots, blocks * width), bf16),
-            dma((3,)), dma((3,)), dma((3,)),
+            dma, dma((3,)), dma((3,)), dma((3,)),
         ]
         + [dma((copies,)) for _ in range(8)]
         + [dma((GROUPS,)) for _ in range(6)],
         compiler_params=pltpu.CompilerParams(
-            collective_id=0, has_side_effects=True, vmem_limit_bytes=48 * 1024 * 1024
+            collective_id=0, has_side_effects=True, vmem_limit_bytes=63 * 1024 * 1024
         ),
     )(
         tokens, norm_gain.reshape(1, features), route_ids.T, route_weights.T,

time: 107 us -> 100 us (0.935); the launches traced: 105 us -> 100 us
  local copies, waits for them, and re-layouts: 7.25 us -> 2.3 us
    unnamed x15 -> x1, local copies, waits for them, and re-layouts: 7.25 us -> 2.3 us
where the time goes in v2:
time: 100 us
  Pallas kernels  97.8 us (98%)
  local copies, waits for them, and re-layouts  2.3 us (2%)
    pallas_call x1, Pallas kernels, group_layer(): pl.pallas_call(functools.partial(group_kernel, members, parts, halves), o...  97.8 us
    unnamed x1, local copies, waits for them, and re-layouts  2.3 us

profile of v2, /device:TPU:9, one launch (start us, length us, event | category | flops | bytes accessed | tf_op | source)
XLA Modules:
  0.0 100.1 jit_solution(16684828372253960290)
XLA Ops:
  0.0 97.8 %shard_map.73 = bf16[256,2048]{1,0:T(8,128)(2,1)} custom-call(bf16[256,2048]{1,0:T(8,128)(2,1)} %tokens.1, f32[1,2048]{1,0:T(1,128)} %bitcast.9, s32[2,256]{1,0:T(2,128)} %bitcast.10, f32[2,256]{1,0:T(2,128)} %bitcast.11, bf16[2048,256]{1,0:T(8,128)(2,1)} %bitcast.6, bf16[2048,256]{1,0:T(8,128)(2,1)} %bitcast.7, bf16[256,2048]{1,0:T(8,128)(2,1)} %bitcast.8), custom_call_target="tpu_custom_call" | custom-call | tf_op jit(solution)/shard_map/pallas_call | solution.py:301
  97.8 2.3 %copy.9 = bf16[256,2048]{1,0:T(8,128)(2,1)} copy(bf16[256,2048]{1,0:T(8,128)(2,1)} %shard_map.73) | data formatting | bytes 2097152

commit v3 on v2

--- a/solution.py
+++ b/solution.py
@@ -8,7 +8,7 @@
 from jax.sharding import PartitionSpec as P
 
 GROUPS = 4
-SPLIT = 2
+SPLIT = 4
 MESH = pl.DeviceIdType.MESH
 
 
@@ -62,9 +62,9 @@
 def group_kernel(
     members, parts, halves,
     tokens, gain, ids, weights, w_gate, w_up, w_down, out,
-    raw, ready, summed, place, sent, taken, scales, scales_in, answers, returned,
+    raw, ready, summed, final, place, sent, taken, scales, scales_in, answers, returned,
     gate_all, up_all, down_all, hidden,
-    raw_sem, own_sems, twin_s, twin_r, peer_s, peer_r, part_s, part_r,
+    raw_sem, out_sems, own_sems, twin_s, twin_r, peer_s, peer_r, part_s, part_r,
     near_s, near_r, far_s, far_r, row_s, row_r, scale_s, scale_r, back_s, back_r,
 ):
     part, position, half = lax.axis_index("grp"), lax.axis_index("ep"), lax.axis_index("tp")
@@ -85,7 +85,6 @@
     neighbours = [peer, other_part, twin] + [level_of(k) for k in range(1, GROUPS)]
     for device in neighbours:
         pl.semaphore_signal(barrier, inc=1, device_id=device, device_id_type=MESH)
-    pl.semaphore_wait(barrier, len(neighbours))
 
     sources = (w_gate, w_up, w_down)
     stores = (gate_all, up_all, down_all)
@@ -127,8 +126,6 @@
     far_copies = [
         spread_copy(i, parts - 1 - part, far_s, far_r, twin) for i in range(len(pieces))
     ]
-    for copy in peer_copies:
-        copy.start()
     own_copies, twin_copies = [], []
     for tensor in range(3):
         own_copies.append(
@@ -140,9 +137,6 @@
                 twin_s.at[tensor], twin_r.at[tensor], twin,
             )
         )
-    for copy in own_copies + twin_copies:
-        copy.start()
-
     first = ids[0:1, :]
     group_row = first // members
     lane = lax.broadcasted_iota(jnp.int32, (8, rows), 0)
@@ -170,8 +164,11 @@
 
     row_copies, scale_copies, back_copies = {}, {}, {}
     slot_iota = lax.broadcasted_iota(jnp.int32, (slots, rows), 0)
+    order = (2, 1, 3, 0)
+    pl.semaphore_wait(barrier, len(neighbours))
+    for copy in peer_copies:
+        copy.start()
     raw_copy.wait()
-    order = (2, 1, 3, 0)
     for k in order:
         key = jnp.where(group_row == (level ^ k), slot_row, -1)
         spots = (jnp.broadcast_to(key, (slots, rows)) == slot_iota).astype(jnp.float32)
@@ -195,6 +192,9 @@
             )
             row_copies[k].start()
             scale_copies[k].start()
+        if k == order[0]:
+            for copy in own_copies + twin_copies:
+                copy.start()
 
     for index in range(len(pieces)):
         peer_copies[index].wait_recv()
@@ -205,20 +205,16 @@
             far_copies[index - 1].start()
     part_copies[-1].wait_recv()
     far_copies[-1].start()
-    for copy in own_copies:
-        copy.wait()
-    for copy in twin_copies + near_copies + far_copies:
-        copy.wait_recv()
 
     width = gate_all.shape[2]
     diagonal = lax.broadcasted_iota(jnp.int32, (slots, slots), 0) == lax.broadcasted_iota(
         jnp.int32, (slots, slots), 1
     )
-    tile = 512
+    tile = features // GROUPS
 
     strip = 32
 
-    def work(k):
+    def norm(k):
         def norm_strip(index, carry):
             window = pl.ds(pl.multiple_of(index * strip, strip), strip)
             floats = taken[k, window, :].astype(jnp.float32)
@@ -227,17 +223,22 @@
             return carry
 
         lax.fori_loop(0, slots // strip, norm_strip, 0)
-        for block in range(members * halves):
-            lanes = scales_in[k][block // halves : block // halves + 1, :]
-            scale = jnp.sum(
-                jnp.where(diagonal, jnp.broadcast_to(lanes, (slots, slots)), 0.0),
-                axis=1, keepdims=True,
-            )
+
+    def widen(k, owner):
+        lanes = scales_in[k, pl.ds(owner, 1), :]
+        scale = jnp.sum(
+            jnp.where(diagonal, jnp.broadcast_to(lanes, (slots, slots)), 0.0),
+            axis=1, keepdims=True,
+        )
+        for side in range(halves):
+            block = owner * halves + side
             gate = jnp.dot(ready[...], gate_all[block], preferred_element_type=jnp.float32)
             up = jnp.dot(ready[...], up_all[block], preferred_element_type=jnp.float32)
-            hidden[:, block * width : (block + 1) * width] = (
+            hidden[:, pl.ds(pl.multiple_of(block * width, width), width)] = (
                 gate / (1.0 + jnp.exp(-gate)) * up * scale
             ).astype(jnp.bfloat16)
+
+    def narrow(k):
         for column in range(features // tile):
             window = slice(column * tile, (column + 1) * tile)
             total = jnp.zeros((slots, tile), jnp.float32)
@@ -252,11 +253,21 @@
             else:
                 returned[0, :, window] = total.astype(jnp.bfloat16)
 
+    for copy in own_copies:
+        copy.wait()
+    for copy in twin_copies:
+        copy.wait_recv()
     for k in order:
         if k:
             row_copies[k].wait_recv()
             scale_copies[k].wait_recv()
-        work(k)
+        norm(k)
+        widen(k, member)
+        if k == order[0]:
+            for copy in near_copies + far_copies:
+                copy.wait_recv()
+        widen(k, members - 1 - member)
+        narrow(k)
         if k:
             back_copies[k] = remote(
                 answers.at[k], returned.at[k], back_s.at[k], back_r.at[k], level_of(k)
@@ -272,12 +283,18 @@
     tiles = [slice(start, start + tile) for start in range(0, features, tile)]
     for window in tiles:
         summed[:, window] = unpack(0, window)
+    out_copies = []
     for k in order[:-1]:
         back_copies[k].wait_recv()
         for window in tiles:
             total = summed[:, window] + unpack(k, window)
             if k == order[-2]:
-                out[:, window] = total.astype(jnp.bfloat16)
+                final[:, window] = total.astype(jnp.bfloat16)
+                copy = pltpu.make_async_copy(
+                    final.at[:, window], out.at[:, window], out_sems.at[window.start // tile]
+                )
+                copy.start()
+                out_copies.append(copy)
             else:
                 summed[:, window] = total
 
@@ -287,6 +304,8 @@
         row_copies[k].wait_send()
         scale_copies[k].wait_send()
         back_copies[k].wait_send()
+    for copy in out_copies:
+        copy.wait()
 
 
 def group_layer(members, tokens, norm_gain, route_ids, route_weights, w_gate, w_up, w_down):
@@ -302,11 +321,12 @@
         functools.partial(group_kernel, members, parts, halves),
         out_shape=jax.ShapeDtypeStruct((rows, features), bf16),
         in_specs=[anywhere] + [vmem] * 3 + [anywhere] * 3,
-        out_specs=vmem,
+        out_specs=anywhere,
         scratch_shapes=[
             pltpu.VMEM((rows, features), bf16),
             pltpu.VMEM((slots, features), bf16),
             pltpu.VMEM((rows, features), f32),
+            pltpu.VMEM((rows, features), bf16),
             pltpu.VMEM((GROUPS * slots, rows), bf16),
             pltpu.VMEM((GROUPS, slots, features), bf16),
             pltpu.VMEM((GROUPS, slots, features), bf16),
@@ -318,7 +338,7 @@
             pltpu.VMEM((blocks, features, width), bf16),
             pltpu.VMEM((blocks, width, features), bf16),
             pltpu.VMEM((slots, blocks * width), bf16),
-            dma, dma((3,)), dma((3,)), dma((3,)),
+            dma, dma((GROUPS,)), dma((3,)), dma((3,)), dma((3,)),
         ]
         + [dma((copies,)) for _ in range(8)]
         + [dma((GROUPS,)) for _ in range(6)],

time: 100 us -> 99.9 us (level); the launches traced: 100 us -> 98.9 us
  Pallas kernels: 97.8 us -> 96.6 us
    pallas_call x1, Pallas kernels: 97.8 us -> 96.6 us  [group_layer(): pl.pallas_call(functools.partial(group_kernel, members, parts, halves), o...]
where the time goes in v3:
time: 99.9 us; the launch traced here: 98.9 us
  Pallas kernels  96.6 us (97%)
  local copies, waits for them, and re-layouts  2.3 us (2%)
    pallas_call x1, Pallas kernels, group_layer(): pl.pallas_call(functools.partial(group_kernel, members, parts, halves), o...  96.6 us
    unnamed x1, local copies, waits for them, and re-layouts  2.3 us

profile of v3, /device:TPU:9, one launch (start us, length us, event | category | flops | bytes accessed | tf_op | source)
XLA Modules:
  0.0 98.9 jit_solution(6331734582495967221)
XLA Ops:
  0.0 96.6 %shard_map.73 = bf16[256,2048]{1,0:T(8,128)(2,1)} custom-call(bf16[256,2048]{1,0:T(8,128)(2,1)} %tokens.1, f32[1,2048]{1,0:T(1,128)} %bitcast.9, s32[2,256]{1,0:T(2,128)} %bitcast.10, f32[2,256]{1,0:T(2,128)} %bitcast.11, bf16[2048,256]{1,0:T(8,128)(2,1)} %bitcast.6, bf16[2048,256]{1,0:T(8,128)(2,1)} %bitcast.7, bf16[256,2048]{1,0:T(8,128)(2,1)} %bitcast.8), custom_call_target="tpu_custom_call" | custom-call | tf_op jit(solution)/shard_map/pallas_call | solution.py:320
  96.6 2.3 %copy.9 = bf16[256,2048]{1,0:T(8,128)(2,1)} copy(bf16[256,2048]{1,0:T(8,128)(2,1)} %shard_map.73) | data formatting | bytes 2097152
